TPU v7x, 32 devices: a whole 2x2x4 slice. The times are simulated.
32 devices in a mesh: grp: 2 (over y), fs: 4 (over z), tp: 4 (over x, core).
Axes of the slice: x: 2, y: 2, z: 4, core: 2. Of those that a mesh axis runs over, the one named last changes fastest.
Arguments:
- tokens: bfloat16 [4096, 2048], P(('grp', 'fs')), parts along dimension 0, may hold values from -6 to 6
- norm_in: bfloat16 [2048], replicated, may hold values from 0.099609375 to 1.8984375
- w_value: bfloat16 [2048, 2048], P('fs', 'tp'), may hold values from -0.125 to 0.125
- w_gate: bfloat16 [2048, 2048], P('fs', 'tp'), may hold values from -0.125 to 0.125
- conv_kernel: float32 [31, 2048], replicated, as said below
- ln_gain: bfloat16 [2048], replicated, may hold values from 0.099609375 to 1.8984375
- ln_shift: bfloat16 [2048], replicated, may hold values from -3 to 3
- w_out: bfloat16 [2048, 2048], P('tp', 'fs'), may hold values from -0.125 to 0.125
- norm_mlp: bfloat16 [2048], replicated, may hold values from 0.099609375 to 1.8984375
- w_up: bfloat16 [2048, 8192], P('fs', 'tp'), may hold values from -0.125 to 0.125
- w_down: bfloat16 [8192, 2048], P('tp', 'fs'), may hold values from -0.0625 to 0.0625
Outputs:
- layer_out: bfloat16 [4096, 2048], P(('grp', 'fs', 'tp')), parts along dimension 0
There are 2 independent parts, one for each index of `grp`. A program takes and returns all parts, laid end to end along the dimension named above; an argument that names none is the same for every part. Nothing has to cross between parts.
Inputs may be any that keep to these rules, and one draw needn't show every extreme that they name: `conv_kernel`: a depthwise kernel.
All inputs are finite; a program needn't handle non-finite values.
Results may differ from a plain program's by a relative error of at most 0.018.
Values may be sent and summed in bfloat16 or wider, within the bound.
A program may use at most 64 MiB of HBM per device.

v0:
```python
import jax
import jax.numpy as jnp
from jax import lax
from jax.sharding import PartitionSpec as P

D = 2048
KERNEL = 31


def rms_scale(values, gain):
    as_float = values.astype(jnp.float32)
    scaled = as_float * lax.rsqrt(jnp.mean(as_float * as_float, axis=-1, keepdims=True) + 1e-06)
    return scaled * gain.astype(jnp.float32)


def shards(
    tokens, norm_in, w_value, w_gate, conv_kernel, ln_gain, ln_shift, w_out, norm_mlp, w_up, w_down
):
    seq_len = tokens.shape[0]
    col_width = w_value.shape[1]
    offset = lax.axis_index("tp") * col_width
    row_share = seq_len // lax.axis_size("tp")
    own_start = lax.axis_index("tp") * row_share
    normed_in = rms_scale(tokens, norm_in).astype(jnp.bfloat16)
    columns = normed_in
    values_f = jnp.dot(
        columns,
        lax.all_gather(w_value, "fs", axis=0, tiled=True),
        preferred_element_type=jnp.float32,
    )
    gate_act = jnp.dot(
        columns,
        lax.all_gather(w_gate, "fs", axis=0, tiled=True),
        preferred_element_type=jnp.float32,
    )
    gated = values_f * jax.nn.sigmoid(gate_act)
    kernel = lax.dynamic_slice_in_dim(conv_kernel, offset, col_width, 1)
    padded = jnp.pad(gated, ((KERNEL - 1, 0), (0, 0)))
    convolved = jnp.zeros_like(gated)
    for tap_index in range(KERNEL):
        convolved = convolved + kernel[tap_index][None, :] * padded[tap_index : tap_index + seq_len]
    stats = lax.psum((jnp.sum(convolved, axis=1), jnp.sum(convolved * convolved, axis=1)), "tp")
    chan_mean = (stats[0] / D)[:, None]
    chan_msq = (stats[1] / D)[:, None]
    variance = chan_msq - chan_mean * chan_mean
    gain_part = lax.dynamic_slice_in_dim(ln_gain, offset, col_width, 0).astype(jnp.float32)
    shift_part = lax.dynamic_slice_in_dim(ln_shift, offset, col_width, 0).astype(jnp.float32)
    normed = (convolved - chan_mean) * lax.rsqrt(variance + 1e-05) * gain_part + shift_part
    activated = jax.nn.silu(normed).astype(jnp.bfloat16)
    partial_value = jnp.dot(
        activated,
        lax.all_gather(w_out, "fs", axis=1, tiled=True),
        preferred_element_type=jnp.float32,
    )
    mixed = lax.psum(partial_value.astype(jnp.bfloat16), "tp").astype(jnp.float32)
    residual = tokens.astype(jnp.float32) + mixed
    normed_mlp = rms_scale(residual, norm_mlp).astype(jnp.bfloat16)
    residual_own = lax.dynamic_slice_in_dim(residual, own_start, row_share, 0)
    columns = normed_mlp
    up_act = jnp.dot(
        columns, lax.all_gather(w_up, "fs", axis=0, tiled=True), preferred_element_type=jnp.float32
    )
    hidden = jnp.square(jax.nn.relu(up_act)).astype(jnp.bfloat16)
    whole_down = lax.all_gather(w_down, "fs", axis=1, tiled=True)
    mlp_own = lax.psum_scatter(
        jnp.dot(hidden, whole_down, preferred_element_type=jnp.float32).astype(jnp.bfloat16),
        "tp",
        scatter_dimension=0,
        tiled=True,
    ).astype(jnp.float32)
    return (residual_own + mlp_own).astype(jnp.bfloat16)


def solution(mesh):
    in_specs = (
        P(("grp", "fs"), None),
        P(),
        P("fs", "tp"),
        P("fs", "tp"),
        P(),
        P(),
        P(),
        P("tp", "fs"),
        P(),
        P("fs", "tp"),
        P("tp", "fs"),
    )
    out_specs = P(("grp", "fs", "tp"), None)
    return jax.shard_map(shards, mesh=mesh, in_specs=in_specs, out_specs=out_specs, check_vma=False)
```

profile of v0, /device:TPU:0, one launch (start us, length us, event | category | flops | bytes accessed | tf_op | source)
XLA Modules:
  0.0 559.9 jit_solution(14983291080787817863)
XLA Ops:
  6.5 0.7 all-gather.8.cloned.1.call-update
  7.3 0.7 all-gather.6.cloned.1.call-update
  8.1 0.7 all-gather.10.cloned.1.call-update
  8.8 0.7 convert_element_type.46
  9.5 0.8 dynamic-slice_convert_fusion
  10.3 1.1 fusion.50
  11.4 1.4 constant_dynamic-slice_fusion
  12.8 2.1 fusion
  14.8 42.5 %all-gather.8.cloned.1.call-done = bf16[2048,512]{1,0:T(8,128)(2,1)} async-done(((bf16[512,512]{1,0:T(8,128)(2,1)}), bf16[2048,512]{1,0:T(8,128)(2,1)}) %all-gather.8.cloned.1.call-update) | async-done | bytes 2097168 | tf_op jit(solution)/shard_map/all_gather | solution.py:33
  57.3 3.0 fusion.7
  60.4 43.0 %all-gather.6.cloned.1.call-done = bf16[2048,512]{1,0:T(8,128)(2,1)} async-done(((bf16[512,512]{1,0:T(8,128)(2,1)}), bf16[2048,512]{1,0:T(8,128)(2,1)}) %all-gather.6.cloned.1.call-update) | async-done | bytes 2097168 | tf_op jit(solution)/shard_map/all_gather | solution.py:28
  103.4 2.9 convolution_multiply_fusion
  106.3 5.0 fusion.49
  111.3 6.8 %all-reduce.1 = (f32[512]{0:T(512)S(1)}, f32[512]{0:T(512)S(1)}) all-reduce(f32[512]{0:T(512)S(1)} %get-tuple-element.6, f32[512]{0:T(512)S(1)} %get-tuple-element.5), channel_id=1, replica_groups=mesh['grp'=2,'fs'=4,'tp'=4] {'tp'}, use_global_device_ids=true, to_apply=%region_4.5 | all-reduce | flops 1024 | bytes 8192 | tf_op jit(solution)/shard_map/psum | solution.py:42
  118.1 31.4 %all-gather.10.cloned.1.call-done = bf16[512,2048]{1,0:T(8,128)(2,1)} async-done(((bf16[512,512]{1,0:T(8,128)(2,1)}), bf16[512,2048]{1,0:T(8,128)(2,1)}) %all-gather.10.cloned.1.call-update) | async-done | bytes 2097168 | tf_op jit(solution)/shard_map/all_gather | solution.py:52
  149.4 4.4 convolution_convert_fusion.1
  153.9 0.5 all-gather.12.cloned.1.call-update
  155.3 48.9 %all-reduce.4.cloned.1.call-done = bf16[512,2048]{1,0:T(8,128)(2,1)} async-done(((bf16[512,2048]{1,0:T(8,128)(2,1)}), bf16[512,2048]{1,0:T(8,128)(2,1)}) %all-reduce.4.cloned.1.call-update) | async-done | bytes 2097168 | tf_op jit(solution)/shard_map/psum | solution.py:55
  204.2 4.2 convert_add_fusion
  208.4 146.9 %all-gather.12.cloned.1.call-done = bf16[2048,2048]{1,0:T(8,128)(2,1)} async-done(((bf16[512,2048]{1,0:T(8,128)(2,1)}), bf16[2048,2048]{1,0:T(8,128)(2,1)}) %all-gather.12.cloned.1.call-update) | async-done | bytes 8388624 | tf_op jit(solution)/shard_map/all_gather | solution.py:61
  355.4 149.3 %all-gather.14.cloned.1.call-done = bf16[2048,2048]{1,0:T(8,128)(2,1)} async-done(((bf16[2048,512]{1,0:T(8,128)(2,1)}), bf16[2048,2048]{1,0:T(8,128)(2,1)}) %all-gather.14.cloned.1.call-update) | async-done | bytes 8388624 | tf_op jit(solution)/shard_map/all_gather | solution.py:64
  504.6 16.6 %convolution_convert_fusion = bf16[512,2048]{1,0:T(8,128)(2,1)} fusion(bf16[2048,2048]{1,0:T(8,128)(2,1)} %all-gather.14.cloned.1.call-done, bf16[2048,2048]{1,0:T(8,128)(2,1)} %all-gather.12.cloned.1.call-done, f32[2048]{0:T(1024)S(1)} %convert_element_type.53, f32[512]{0:T(512)S(1)} %add_rsqrt_fusion, bf16[512,2048]{1,0:T(8,128)(2,1)S(1)} %copy-done, ...), kind=kOutput, calls=%fused_computation.9 | convolution fusion | flops 8600420352 | bytes 23078912 | tf_op jit(solution)/shard_map/dot_general | solution.py:66
  521.2 29.5 %reduce-scatter.2.cloned.1.call-done = bf16[128,2048]{1,0:T(8,128)(2,1)} async-done(((bf16[512,2048]{1,0:T(8,128)(2,1)}), bf16[128,2048]{1,0:T(8,128)(2,1)}) %reduce-scatter.2.cloned.1.call-update) | async-done | bytes 524304 | tf_op jit(solution)/shard_map/reduce_scatter | solution.py:65
  550.8 2.3 add_convert_fusion
  (18 shorter events, 1.0 us)
Async XLA Ops:
  6.5 50.8 %copy-start = (bf16[512,2048]{1,0:T(8,128)(2,1)S(1)}, bf16[512,2048]{1,0:T(8,128)(2,1)}, u32[]{:S(2)}) copy-start(bf16[512,2048]{1,0:T(8,128)(2,1)} %param.11) | copy-start | bytes 6291460
  6.5 50.8 %all-gather.8.cloned.1.call-start = ((), (), s32[]{:S(2)}) async-start(), calls=%async_computation.2 | async-start | bytes 2621440 | tf_op jit(solution)/shard_map/all_gather | solution.py:33
  7.3 96.1 %all-gather.6.cloned.1.call-start = ((), (), s32[]{:S(2)}) async-start(), calls=%async_computation.1 | async-start | bytes 2621440 | tf_op jit(solution)/shard_map/all_gather | solution.py:28
  8.0 141.4 %all-gather.10.cloned.1.call-start = ((), (), s32[]{:S(2)}) async-start(), calls=%async_computation.3 | async-start | bytes 2621440 | tf_op jit(solution)/shard_map/all_gather | solution.py:52
  8.7 195.5 %all-reduce.4.cloned.1.call-start = ((), (), s32[]{:S(2)}) async-start(), calls=%async_computation.4 | async-start | bytes 4194304 | tf_op jit(solution)/shard_map/psum | solution.py:55
  153.9 1.4 copy-start.1
  153.9 201.5 %all-gather.12.cloned.1.call-start = ((), (), s32[]{:S(2)}) async-start(), calls=%async_computation.5 | async-start | bytes 10485760 | tf_op jit(solution)/shard_map/all_gather | solution.py:61
  154.5 350.1 %all-gather.14.cloned.1.call-start = ((), (), s32[]{:S(2)}) async-start(), calls=%async_computation.6 | async-start | bytes 10485760 | tf_op jit(solution)/shard_map/all_gather | solution.py:64
  155.1 395.7 %reduce-scatter.2.cloned.1.call-start = ((), (), s32[]{:S(2)}) async-start(), calls=%async_computation.7 | async-start | bytes 2621440 | tf_op jit(solution)/shard_map/reduce_scatter | solution.py:65
Sparse Core Ops, SparseCore 0:
  8.9 48.3 all-gather.7
  58.9 44.4 all-gather.5
  105.0 44.4 all-gather.9
  154.0 50.1 all-reduce.3
  205.6 149.6 all-gather.11
  356.8 147.7 all-gather.13
  521.4 29.3 reduce-scatter.1
where the time goes:
time: 560 us
  waiting for transfers between devices  495 us (88%)
  matrix products  26.9 us (5%)
  other arithmetic  15 us (3%)
  between operations  13.6 us (2%)
  blocking collectives  6.79 us (1%)
    all_gather x1, waiting for transfers between devices, shards(): whole_down = lax.all_gather(w_down, 'fs', axis=1, tiled=True)  149 us
    all_gather x1, waiting for transfers between devices, shards(): lax.all_gather(w_up, 'fs', axis=0, tiled=True)  147 us
    psum x1, waiting for transfers between devices, shards(): lax.psum(partial_value.astype(jnp.bfloat16), 'tp').astype(jnp.float32)  48.9 us
    all_gather x1, waiting for transfers between devices, shards(): lax.all_gather(w_value, 'fs', axis=0, tiled=True)  43 us
    all_gather x1, waiting for transfers between devices, shards(): lax.all_gather(w_gate, 'fs', axis=0, tiled=True)  42.5 us
    all_gather x1, waiting for transfers between devices, shards(): lax.all_gather(w_out, 'fs', axis=1, tiled=True)  31.4 us
    reduce_scatter x1, waiting for transfers between devices, shards(): lax.psum_scatter(jnp.dot(hidden, whole_down, preferred_element_type=jnp.f...  29.5 us
    dot_general x1, matrix products, shards(): jnp.dot(hidden, whole_down, preferred_element_type=jnp.float32)  16.6 us
  transfers between devices with their start and end apart: 7, of which 7 were waited for; matrix products, arithmetic and copies ran while one was open for 4% of the time, Pallas kernels for 0%

commit v1 on v0

--- a/solution.py
+++ b/solution.py
@@ -61,7 +61,7 @@
         columns, lax.all_gather(w_up, "fs", axis=0, tiled=True), preferred_element_type=jnp.float32
     )
     hidden = jnp.square(jax.nn.relu(up_act)).astype(jnp.bfloat16)
-    whole_down = lax.all_gather(w_down, "fs", axis=1, tiled=True)
+    whole_down = jnp.concatenate(lax.all_gather(w_down, "fs"), axis=1)
     mlp_own = lax.psum_scatter(
         jnp.dot(hidden, whole_down, preferred_element_type=jnp.float32).astype(jnp.bfloat16),
         "tp",

time: 560 us -> 561 us (level)
  waiting for transfers between devices: 495 us -> 482 us
  local copies, waits for them, and re-layouts: 2.49 us -> 14.2 us
    reshape x0 -> x1, local copies, waits for them, and re-layouts: none -> 11.8 us  [shards(): whole_down = jnp.concatenate(lax.all_gather(w_down, 'fs'), axis=1)]
    all_gather x1, waiting for transfers between devices: 147 us -> 137 us  [shards(): lax.all_gather(w_up, 'fs', axis=0, tiled=True)]
  transfers between devices with their start and end apart: 7 -> 7, of which waited for: 7 -> 7; matrix products, arithmetic and copies ran while one was open for 4% -> 6% of each run, Pallas kernels for 0% -> 0%
where the time goes in v1:
time: 561 us; the launch traced here: 560 us
  waiting for transfers between devices  482 us (86%)
  matrix products  28.2 us (5%)
  other arithmetic  15.1 us (3%)
  local copies, waits for them, and re-layouts  14.2 us (3%)
  between operations  13.6 us (2%)
  blocking collectives  6.81 us (1%)
    all_gather x1, waiting for transfers between devices, shards(): whole_down = jnp.concatenate(lax.all_gather(w_down, 'fs'), axis=1)  147 us
    all_gather x1, waiting for transfers between devices, shards(): lax.all_gather(w_up, 'fs', axis=0, tiled=True)  137 us
    psum x1, waiting for transfers between devices, shards(): lax.psum(partial_value.astype(jnp.bfloat16), 'tp').astype(jnp.float32)  48.9 us
    all_gather x1, waiting for transfers between devices, shards(): lax.all_gather(w_gate, 'fs', axis=0, tiled=True)  42.5 us
    all_gather x1, waiting for transfers between devices, shards(): lax.all_gather(w_value, 'fs', axis=0, tiled=True)  42 us
    all_gather x1, waiting for transfers between devices, shards(): lax.all_gather(w_out, 'fs', axis=1, tiled=True)  31.1 us
    reduce_scatter x1, waiting for transfers between devices, shards(): lax.psum_scatter(jnp.dot(hidden, whole_down, preferred_element_type=jnp.f...  29.5 us
    dot_general x1, matrix products, shards(): jnp.dot(hidden, whole_down, preferred_element_type=jnp.float32)  16.6 us
  transfers between devices with their start and end apart: 7, of which 7 were waited for; matrix products, arithmetic and copies ran while one was open for 6% of the time, Pallas kernels for 0%

profile of v1, /device:TPU:0, one launch (start us, length us, event | category | flops | bytes accessed | tf_op | source)
XLA Modules:
  0.0 559.9 jit_solution(4631700407277298017)
XLA Ops:
  6.5 0.7 all-gather.9.cloned.1.call-update
  7.3 0.7 all-gather.7.cloned.1.call-update
  8.1 0.7 all-gather.11.cloned.1.call-update
  8.8 0.7 convert_element_type.46
  9.5 0.8 dynamic-slice_convert_fusion
  10.3 1.2 fusion.50
  11.5 1.2 constant_dynamic-slice_fusion
  12.7 2.1 fusion
  14.8 42.5 %all-gather.9.cloned.1.call-done = bf16[2048,512]{1,0:T(8,128)(2,1)} async-done(((bf16[512,512]{1,0:T(8,128)(2,1)}), bf16[2048,512]{1,0:T(8,128)(2,1)}) %all-gather.9.cloned.1.call-update) | async-done | bytes 2097168 | tf_op jit(solution)/shard_map/all_gather | solution.py:33
  57.3 4.0 fusion.7
  61.3 42.0 %all-gather.7.cloned.1.call-done = bf16[2048,512]{1,0:T(8,128)(2,1)} async-done(((bf16[512,512]{1,0:T(8,128)(2,1)}), bf16[2048,512]{1,0:T(8,128)(2,1)}) %all-gather.7.cloned.1.call-update) | async-done | bytes 2097168 | tf_op jit(solution)/shard_map/all_gather | solution.py:28
  103.4 3.1 convolution_multiply_fusion
  106.5 5.0 fusion.49
  111.5 6.8 %all-reduce.1 = (f32[512]{0:T(512)S(1)}, f32[512]{0:T(512)S(1)}) all-reduce(f32[512]{0:T(512)S(1)} %get-tuple-element.6, f32[512]{0:T(512)S(1)} %get-tuple-element.5), channel_id=1, replica_groups=mesh['grp'=2,'fs'=4,'tp'=4] {'tp'}, use_global_device_ids=true, to_apply=%region_4.5 | all-reduce | flops 1024 | bytes 8192 | tf_op jit(solution)/shard_map/psum | solution.py:42
  118.3 31.1 %all-gather.11.cloned.1.call-done = bf16[512,2048]{1,0:T(8,128)(2,1)} async-done(((bf16[512,512]{1,0:T(8,128)(2,1)}), bf16[512,2048]{1,0:T(8,128)(2,1)}) %all-gather.11.cloned.1.call-update) | async-done | bytes 2097168 | tf_op jit(solution)/shard_map/all_gather | solution.py:52
  149.5 4.4 convolution_convert_fusion.1
  155.3 48.9 %all-reduce.4.cloned.1.call-done = bf16[512,2048]{1,0:T(8,128)(2,1)} async-done(((bf16[512,2048]{1,0:T(8,128)(2,1)}), bf16[512,2048]{1,0:T(8,128)(2,1)}) %all-reduce.4.cloned.1.call-update) | async-done | bytes 2097168 | tf_op jit(solution)/shard_map/psum | solution.py:55
  204.2 4.2 convert_add_fusion
  208.5 146.9 %all-gather.15.cloned.1.call-done = bf16[8192,512]{1,0:T(8,128)(2,1)} async-done(((bf16[2048,512]{1,0:T(8,128)(2,1)}), bf16[8192,512]{1,0:T(8,128)(2,1)}) %all-gather.15.cloned.1.call-update) | async-done | bytes 8388624 | tf_op jit(solution)/shard_map/all_gather | solution.py:64
  355.4 11.8 %copy.12 = bf16[2048,4,512]{0,2,1:T(8,128)(2,1)} copy(bf16[2048,4,512]{2,0,1:T(8,128)(2,1)} %bitcast.45) | data formatting | bytes 16777216 | tf_op jit(solution)/shard_map/reshape | solution.py:64
  367.1 137.5 %all-gather.13.cloned.1.call-done = bf16[2048,2048]{1,0:T(8,128)(2,1)} async-done(((bf16[512,2048]{1,0:T(8,128)(2,1)}), bf16[2048,2048]{1,0:T(8,128)(2,1)}) %all-gather.13.cloned.1.call-update) | async-done | bytes 8388624 | tf_op jit(solution)/shard_map/all_gather | solution.py:61
  504.6 16.6 %convolution_convert_fusion = bf16[512,2048]{1,0:T(8,128)(2,1)} fusion(bf16[2048,2048]{0,1:T(8,128)(2,1)} %bitcast.46, bf16[2048,2048]{1,0:T(8,128)(2,1)} %all-gather.13.cloned.1.call-done, f32[2048]{0:T(1024)S(1)} %convert_element_type.53, f32[512]{0:T(512)S(1)} %add_rsqrt_fusion, bf16[512,2048]{1,0:T(8,128)(2,1)S(1)} %copy-done, ...), kind=kOutput, calls=%fused_computation.9 | convolution fusion | flops 8600420352 | bytes 23078912 | tf_op jit(solution)/shard_map/dot_general | solution.py:66
  521.2 29.5 %reduce-scatter.2.cloned.1.call-done = bf16[128,2048]{1,0:T(8,128)(2,1)} async-done(((bf16[512,2048]{1,0:T(8,128)(2,1)}), bf16[128,2048]{1,0:T(8,128)(2,1)}) %reduce-scatter.2.cloned.1.call-update) | async-done | bytes 524304 | tf_op jit(solution)/shard_map/reduce_scatter | solution.py:65
  550.8 2.3 add_convert_fusion
  (19 shorter events, 1.5 us)
Async XLA Ops:
  6.5 50.8 %copy-start = (bf16[512,2048]{1,0:T(8,128)(2,1)S(1)}, bf16[512,2048]{1,0:T(8,128)(2,1)}, u32[]{:S(2)}) copy-start(bf16[512,2048]{1,0:T(8,128)(2,1)} %param.11) | copy-start | bytes 6291460
  6.5 50.8 %all-gather.9.cloned.1.call-start = ((), (), s32[]{:S(2)}) async-start(), calls=%async_computation.2 | async-start | bytes 2621440 | tf_op jit(solution)/shard_map/all_gather | solution.py:33
  7.3 96.1 %all-gather.7.cloned.1.call-start = ((), (), s32[]{:S(2)}) async-start(), calls=%async_computation.1 | async-start | bytes 2621440 | tf_op jit(solution)/shard_map/all_gather | solution.py:28
  8.0 141.4 %all-gather.11.cloned.1.call-start = ((), (), s32[]{:S(2)}) async-start(), calls=%async_computation.3 | async-start | bytes 2621440 | tf_op jit(solution)/shard_map/all_gather | solution.py:52
  8.7 195.5 %all-reduce.4.cloned.1.call-start = ((), (), s32[]{:S(2)}) async-start(), calls=%async_computation.4 | async-start | bytes 4194304 | tf_op jit(solution)/shard_map/psum | solution.py:55
  153.9 1.4 copy-start.1
  153.9 201.5 %all-gather.15.cloned.1.call-start = ((), (), s32[]{:S(2)}) async-start(), calls=%async_computation.7 | async-start | bytes 10485760 | tf_op jit(solution)/shard_map/all_gather | solution.py:64
  154.5 350.1 %all-gather.13.cloned.1.call-start = ((), (), s32[]{:S(2)}) async-start(), calls=%async_computation.5 | async-start | bytes 10485760 | tf_op jit(solution)/shard_map/all_gather | solution.py:61
  155.1 395.7 %reduce-scatter.2.cloned.1.call-start = ((), (), s32[]{:S(2)}) async-start(), calls=%async_computation.6 | async-start | bytes 2621440 | tf_op jit(solution)/shard_map/reduce_scatter | solution.py:65
Sparse Core Ops, SparseCore 0:
  8.9 48.3 all-gather.8
  58.9 44.4 all-gather.6
  105.0 44.4 all-gather.10
  154.0 50.1 all-reduce.3
  205.6 149.6 all-gather.14
  356.8 147.7 all-gather.12
  521.4 29.3 reduce-scatter.1
